TPU v7x, 32 devices: a whole 2x2x4 slice. The times are simulated.
32 devices in a mesh: ep: 8 (over z, y), tp: 4 (over x, core).
Axes of the slice: x: 2, y: 2, z: 4, core: 2. Of those that a mesh axis runs over, the one named last changes fastest.
Arguments:
- mixer_input: bfloat16 [4096, 2048], P('ep'), may hold values from -6 to 6
- log_forget_total: float32 [16, 4096], P('tp'), may hold values from -684 to 0, as said below
- mixer_gain: float32 [2048], replicated, may hold values from 0.1 to 1.9
- w_query: bfloat16 [2048, 1024], P(None, 'tp'), may hold values from -1 to 1
- w_key: bfloat16 [2048, 256], P(None, 'tp'), may hold values from -8 to 8
- w_value: bfloat16 [2048, 256], P(None, 'tp'), may hold values from -0.125 to 0.125
- w_output: bfloat16 [1024, 2048], replicated, may hold values from -0.1875 to 0.1875
- mixer_post_gain: float32 [2048], replicated, may hold values from 0.1 to 1.9
- expert_input: bfloat16 [2048, 2048], P('ep'), may hold values from -6 to 6
- expert_ids: int32 [2048, 2], P('ep'), may hold values from 0 to 7, all different within a row; in each aligned block of 64 rows (0 to 63, 64 to 127, ...) at most 32 rows name the same one
- route_weight: float32 [2048, 2], P('ep'), may hold values from 0.1 to 1
- expert_gain: float32 [2048], replicated, may hold values from 0.1 to 1.9
- w_gate: bfloat16 [8, 2048, 3584], P('ep', None, 'tp'), may hold values from -0.125 to 0.125
- w_up: bfloat16 [8, 2048, 3584], P('ep', None, 'tp'), may hold values from -0.125 to 0.125
- w_down: bfloat16 [8, 3584, 2048], P('ep', 'tp'), may hold values from -0.09375 to 0.09375
- expert_post_gain: float32 [2048], replicated, may hold values from 0.1 to 1.9
Outputs:
- mixer_out: bfloat16 [4096, 2048], P(('ep', 'tp'))
- expert_out: bfloat16 [2048, 2048], P(('ep', 'tp'))
Inputs may be any that keep to these rules, and one draw needn't show every extreme that they name: `expert_ids`: in each aligned block of 64 tokens no expert is named by more than 32 of them. `log_forget_total`: each head's values never rise along the positions.
All inputs are finite; a program needn't handle non-finite values.
Results may differ from a plain program's by a relative error of at most 0.012.
The roundings to bfloat16 on the way count: a program that leaves them out, or rounds other values in their place, can miss the bound.
Values may be sent and summed in bfloat16 or wider, within the bound.
A program may use at most 128 MiB of HBM per device.

v0:
```python
import math
import jax
import jax.numpy as jnp
from jax import lax
from jax.sharding import PartitionSpec as P

HD = 64
TOP_K = 2
NEG_FILL = -1e30
NORM_EPS = 1e-06


def norm_rows(values_in, gain_vec):
    widened = values_in.astype(jnp.float32)
    return (
        widened
        * lax.rsqrt(jnp.mean(widened * widened, axis=-1, keepdims=True) + NORM_EPS)
        * gain_vec
    )


def unchanged(present_state):
    return present_state


def mixer_half(
    mixer_input, log_forget_total, mixer_gain, w_query, w_key, w_value, w_output, mixer_post_gain
):
    row_count = mixer_input.shape[0]
    offset = lax.axis_index("ep") * row_count
    head_local = w_query.shape[1] // HD
    kv_local = w_key.shape[1] // HD
    group_size = head_local // kv_local
    normed = norm_rows(mixer_input, mixer_gain).astype(jnp.bfloat16)
    queries = (
        jnp.dot(normed, w_query, preferred_element_type=jnp.float32)
        .astype(jnp.bfloat16)
        .reshape(row_count, kv_local, group_size, HD)
    )
    key_rows = (
        jnp.dot(normed, w_key, preferred_element_type=jnp.float32)
        .astype(jnp.bfloat16)
        .reshape(row_count, kv_local, HD)
    )
    value_rows = (
        jnp.dot(normed, w_value, preferred_element_type=jnp.float32)
        .astype(jnp.bfloat16)
        .reshape(row_count, kv_local, HD)
    )
    gate_totals = log_forget_total.reshape(kv_local, group_size, -1)
    query_gate = lax.dynamic_slice_in_dim(gate_totals, offset, row_count, 2)
    query_pos = offset + jnp.arange(row_count, dtype=jnp.int32)
    last_row = offset + row_count - 1
    score_scale = HD ** (-0.5)
    start_state = (
        jnp.full((kv_local, group_size, row_count), NEG_FILL, jnp.float32),
        jnp.zeros((kv_local, group_size, row_count), jnp.float32),
        jnp.zeros((kv_local, group_size, row_count, HD), jnp.float32),
    )
    running = start_state
    key_piece = lax.all_gather(key_rows, "ep", axis=0, tiled=True)
    value_piece = lax.all_gather(value_rows, "ep", axis=0, tiled=True)
    piece_rows = key_piece.shape[0]
    block_rows = math.gcd(piece_rows, 512)
    block_total = piece_rows // block_rows
    key_blocks = key_piece.reshape(block_total, block_rows, kv_local, HD)
    value_blocks = value_piece.reshape(block_total, block_rows, kv_local, HD)

    def one_block(present_state, operands):
        key_block, value_block, block_index = operands
        block_first = block_index * block_rows

        def update(prior_value):
            row_max, denominator, numerator = prior_value
            key_gate = lax.dynamic_slice_in_dim(gate_totals, block_first, block_rows, 2)
            scores = (
                jnp.einsum("qgjd,kgd->gjqk", queries, key_block, preferred_element_type=jnp.float32)
                * score_scale
            )
            scores = scores + query_gate[:, :, :, None] - key_gate[:, :, None, :]
            visible = (block_first + jnp.arange(block_rows, dtype=jnp.int32))[None, :] <= query_pos[
                :, None
            ]
            scores = jnp.where(visible, scores, NEG_FILL)
            new_max = jnp.maximum(row_max, jnp.max(scores, axis=-1))
            shifted = jnp.where(visible, jnp.exp(scores - new_max[..., None]), 0.0)
            factor = jnp.exp(row_max - new_max)
            denominator = denominator * factor + jnp.sum(shifted, axis=-1)
            numerator = numerator * factor[..., None] + jnp.einsum(
                "gjqk,kgd->gjqd",
                shifted.astype(jnp.bfloat16),
                value_block,
                preferred_element_type=jnp.float32,
            )
            return (new_max, denominator, numerator)

        return (lax.cond(block_first <= last_row, update, unchanged, present_state), None)

    running, _ = lax.scan(
        one_block, running, (key_blocks, value_blocks, jnp.arange(block_total, dtype=jnp.int32))
    )
    row_max, denominator, numerator = running
    mixed_heads = (
        jnp.transpose(numerator / denominator[..., None], (2, 0, 1, 3))
        .reshape(row_count, head_local * HD)
        .astype(jnp.bfloat16)
    )
    by_rows = lax.all_to_all(mixed_heads, "tp", split_axis=0, concat_axis=1, tiled=True)
    projected = jnp.dot(by_rows, w_output, preferred_element_type=jnp.float32)
    return norm_rows(projected, mixer_post_gain).astype(jnp.bfloat16)


def expert_half(
    expert_input, expert_ids, route_weight, expert_gain, w_gate, w_up, w_down, expert_post_gain
):
    row_count = expert_input.shape[0]
    quarters = lax.axis_size("tp")
    experts = lax.axis_size("ep")
    quarter_rows = row_count // quarters
    slot_count = 2 * TOP_K * quarter_rows // experts
    own_quarter = lax.axis_index("tp")
    normed = norm_rows(expert_input, expert_gain).astype(jnp.bfloat16)
    padded_rows = jnp.concatenate([normed, jnp.zeros((1, normed.shape[1]), jnp.bfloat16)], axis=0)
    routed = expert_ids.reshape(quarters, quarter_rows * TOP_K)
    matches = (routed[:, :, None] == jnp.arange(experts, dtype=jnp.int32)[None, None, :]).astype(
        jnp.int32
    )
    slot_ranks = jnp.sum(jnp.cumsum(matches, axis=1) * matches, axis=2) - 1
    owners = (jnp.arange(row_count * TOP_K, dtype=jnp.int32) // TOP_K).reshape(
        quarters, quarter_rows * TOP_K
    )
    quarter_index = jnp.broadcast_to(jnp.arange(quarters, dtype=jnp.int32)[:, None], routed.shape)
    slot_table = (
        jnp.full((quarters, slot_count, experts), row_count, jnp.int32)
        .at[quarter_index, slot_ranks, routed]
        .set(owners)
    )
    gate_local = w_gate[0]
    up_local = w_up[0]
    down_local = w_down[0]
    unit_count = gate_local.shape[1]
    own_table = lax.dynamic_index_in_dim(slot_table, own_quarter, 0, keepdims=False)
    outgoing = padded_rows[own_table]
    arrived = lax.all_to_all(outgoing, "ep", split_axis=1, concat_axis=1, tiled=True)
    slot_rows = lax.all_gather(arrived[None], "tp", axis=0, tiled=True)
    flat_rows = slot_rows.reshape(-1, slot_rows.shape[-1])
    gate_part = jnp.dot(flat_rows, gate_local, preferred_element_type=jnp.float32)
    up_part = jnp.dot(flat_rows, up_local, preferred_element_type=jnp.float32)
    hidden = (
        (jax.nn.silu(gate_part) * up_part)
        .astype(jnp.bfloat16)
        .reshape(slot_rows.shape[:-1] + (unit_count,))
    )
    product = jnp.dot(
        hidden.reshape(-1, unit_count), down_local, preferred_element_type=jnp.float32
    )
    summed = lax.psum_scatter(
        product.reshape(lax.axis_size("tp") * 1, slot_count, experts, product.shape[-1]).astype(
            jnp.bfloat16
        ),
        "tp",
        scatter_dimension=0,
        tiled=True,
    ).astype(jnp.float32)
    results = summed[0].astype(jnp.bfloat16)
    returned = lax.all_to_all(results, "ep", split_axis=1, concat_axis=1, tiled=True)
    flat_results = returned.reshape(slot_count * experts, returned.shape[-1])
    own_routes = lax.dynamic_index_in_dim(routed, own_quarter, 0, keepdims=False)
    own_ranks = lax.dynamic_index_in_dim(slot_ranks, own_quarter, 0, keepdims=False)
    picked = flat_results[own_ranks * experts + own_routes].reshape(quarter_rows, TOP_K, -1)
    own_weights = lax.dynamic_slice_in_dim(
        route_weight, own_quarter * quarter_rows, quarter_rows, 0
    )
    combined = jnp.sum(own_weights[:, :, None] * picked.astype(jnp.float32), axis=1)
    return norm_rows(combined, expert_post_gain).astype(jnp.bfloat16)


def per_device(
    mixer_input,
    log_forget_total,
    mixer_gain,
    w_query,
    w_key,
    w_value,
    w_output,
    mixer_post_gain,
    expert_input,
    expert_ids,
    route_weight,
    expert_gain,
    w_gate,
    w_up,
    w_down,
    expert_post_gain,
):
    mixer_out = mixer_half(
        mixer_input,
        log_forget_total,
        mixer_gain,
        w_query,
        w_key,
        w_value,
        w_output,
        mixer_post_gain,
    )
    expert_out = expert_half(
        expert_input, expert_ids, route_weight, expert_gain, w_gate, w_up, w_down, expert_post_gain
    )
    return (mixer_out, expert_out)


def solution(mesh):
    placed = (
        P("ep", None),
        P("tp", None),
        P(),
        P(None, "tp"),
        P(None, "tp"),
        P(None, "tp"),
        P(),
        P(),
        P("ep", None),
        P("ep", None),
        P("ep", None),
        P(),
        P("ep", None, "tp"),
        P("ep", None, "tp"),
        P("ep", "tp", None),
        P(),
    )
    return jax.shard_map(
        per_device,
        mesh=mesh,
        in_specs=placed,
        out_specs=(P(("ep", "tp"), None), P(("ep", "tp"), None)),
        check_vma=False,
    )
```

profile of v0, /device:TPU:0, one launch (start us, length us, event | category | flops | bytes accessed | tf_op | source)
XLA Modules:
  0.0 324.2 jit_solution(3863174267052389493)
XLA Ops:
  7.2 0.9 copy.41
  8.2 0.1 eq.15
  8.3 0.1 reshape.284
  8.5 0.1 fusion.46
  8.7 0.3 reduce_window_sum.11
  8.9 0.2 select_reduce_fusion
  9.2 29.5 %scatter_fusion = s32[4,32,8]{1,2,0:T(8,128)S(1)} fusion(s32[4,32,8]{1,2,0:T(8,128)S(1)} %broadcast_in_dim.39, s32[512]{0:T(512)S(1)} %fusion.52, s32[512]{0:T(512)S(1)} %fusion.54), kind=kCustom, calls=%fused_computation.2 | custom fusion | bytes 12288 | tf_op jit(solution)/shard_map/scatter | solution.py:136
  38.8 0.1 copy.43
  38.8 0.1 reshape.290
  39.0 0.3 fusion.43
  39.3 0.3 fusion.45
  39.6 0.1 concatenate.6
  39.7 1.4 gather_fusion
  41.0 0.6 copy.44
  41.6 32.9 %all_to_all.26 = bf16[32,8,2048]{2,0,1:T(8,128)(2,1)S(1)} all-to-all(bf16[32,8,2048]{2,0,1:T(8,128)(2,1)S(1)} %copy.44), channel_id=1, replica_groups=mesh['ep'=8,'tp'=4] {'ep'}, dimensions={1} | all-to-all | bytes 2097152 | tf_op jit(solution)/shard_map/all_to_all | solution.py:144
  74.5 1.6 copy.45
  76.1 0.2 reduce-scatter.2.cloned.1.call-start
  76.3 33.4 %all-gather.5.cloned.1.call-done = bf16[128,8,2048]{2,1,0:T(8,128)(2,1)} async-done(((bf16[32,8,2048]{2,1,0:T(8,128)(2,1)}), bf16[128,8,2048]{2,1,0:T(8,128)(2,1)}) %all-gather.5.cloned.1.call-update) | async-done | bytes 4194320 | tf_op jit(solution)/shard_map/all_gather | solution.py:145
  109.7 7.5 %fusion.32 = f32[1024,896]{1,0:T(8,128)S(1)} fusion(bf16[128,8,2048]{2,1,0:T(8,128)(2,1)} %all-gather.5.cloned.1.call-done, bf16[1,2048,896]{2,1,0:T(8,128)(2,1)} %param.33), kind=kOutput, calls=%fused_computation.40 | convolution fusion | flops 3758096384 | bytes 11534336 | tf_op jit(solution)/shard_map/dot_general | solution.py:148
  117.2 4.8 %multiply_convert_fusion = bf16[1024,896]{1,0:T(8,128)(2,1)S(1)} fusion(f32[1024,896]{1,0:T(8,128)S(1)} %fusion.32, bf16[1,2048,896]{2,1,0:T(8,128)(2,1)S(1)} %copy-done.11, bf16[128,8,2048]{2,1,0:T(8,128)(2,1)S(1)} %copy-done.10), kind=kOutput, calls=%fused_computation.48 | convolution fusion | flops 3763601408 | bytes 13369344 | tf_op jit(solution)/shard_map/dot_general | solution.py:147
  122.0 6.0 %convolution_convert_fusion = bf16[4,32,8,2048]{3,2,1,0:T(8,128)(2,1)} fusion(bf16[4,32,8,896]{3,2,1,0:T(8,128)(2,1)S(1)} %bitcast.163, bf16[1,896,2048]{2,1,0:T(8,128)(2,1)S(1)} %copy-done.12), kind=kOutput, calls=%fused_computation.44 | convolution fusion | flops 3760193536 | bytes 9699328 | tf_op jit(solution)/shard_map/dot_general | solution.py:154
  128.0 1.5 copy-done.1
  129.6 0.5 fusion.29
  130.1 2.2 fusion.31
  132.3 0.8 convolution_convert_fusion.3
  133.0 31.5 %all-gather = bf16[4096,64]{0,1:T(8,128)(2,1)S(1)} all-gather(bf16[512,64]{0,1:T(8,128)(2,1)S(1)} %convolution_convert_fusion.3), channel_id=2, replica_groups=mesh['ep'=8,'tp'=4] {'ep'}, dimensions={0}, use_global_device_ids=true | all-gather | bytes 589824 | tf_op jit(solution)/shard_map/all_gather | solution.py:61
  164.5 0.2 copy.50
  164.7 0.9 copy.37
  165.6 0.8 convolution_convert_fusion.2
  166.4 31.4 %all-gather.1 = bf16[4096,64]{0,1:T(8,128)(2,1)S(1)} all-gather(bf16[512,64]{0,1:T(8,128)(2,1)S(1)} %convolution_convert_fusion.2), channel_id=3, replica_groups=mesh['ep'=8,'tp'=4] {'ep'}, dimensions={0}, use_global_device_ids=true | all-gather | bytes 589824 | tf_op jit(solution)/shard_map/all_gather | solution.py:62
  197.8 0.2 copy.51
  198.0 1.0 copy.38
  199.0 0.7 dynamic-slice_bitcast_fusion.1
  199.7 1.5 convolution_convert_fusion.1
  201.2 18.1 %while.15 = (s32[]{:T(128)}, f32[1,4,512]{2,1,0:T(4,128)S(1)}, f32[1,4,512]{2,1,0:T(4,128)S(1)}, f32[1,4,512,64]{2,3,1,0:T(8,128)S(1)}, s32[8]{0:T(128)S(1)}, /*...) while((s32[]{:T(128)}, f32[1,4,512]{2,1,0:T(4,128)S(1)}, ...), condition=%wide.region_6.7_spmd.clone, body=%wide.region_1.6_spmd.clone.sunk | while | flops 288889856 | bytes 15283569 | solution.py:99
  201.2 0.7 dynamic_slice.79
  202.5 7.4 %conditional.3 = ((f32[1,4,512]{2,1,0:T(4,128)S(1)}, f32[1,4,512]{2,1,0:T(4,128)S(1)}, f32[1,4,512,64]{2,3,1,0:T(8,128)S(1)})) conditional(s32[]{:T(128)} %convert_element_type.123, (f32[1,4,512]{2,1,0:T(4,128)S(1)}, f32[1,4,512]{2,1,0:T(4,128)S(1)}, f32[1,4,512,64]{2,3,1,0:T(8,128)S(1)}) %tuple.48, (s32[]{:T(128)}, s32[]{:T(128)}, ...), branch_computations={%region_2.2_spmd, %region_3.5_spmd} | conditional | flops 288889856 | bytes 15281230 | solution.py:97
  202.5 0.8 dynamic-slice_bitcast_fusion
  203.3 0.2 broadcast_compare_fusion
  203.6 2.2 fusion.6
  205.8 2.6 fusion.14
  208.4 1.5 fusion.5
  210.0 0.7 dynamic_slice.79
  211.3 0.7 dynamic_slice.79
  212.6 0.7 dynamic_slice.79
  214.0 0.7 dynamic_slice.79
  215.3 0.7 dynamic_slice.79
  216.7 0.7 dynamic_slice.79
  218.0 0.7 dynamic_slice.79
  219.5 0.7 copy.39
  220.2 3.4 %all-to-all-start = ((bf16[4,128,256]{1,2,0:T(8,128)(2,1)}), bf16[4,128,256]{1,2,0:T(8,128)(2,1)S(1)}, u32[]{:S(2)}, u32[]{:S(2)}) async-start(bf16[4,128,256]{1,2,0:T(8,128)(2,1)} %copy.39), calls=%async_computation | async-start | bytes 524288 | tf_op jit(solution)/shard_map/all_to_all | solution.py:108
  223.7 2.8 copy.46
  226.5 3.1 all-to-all-done
  229.6 57.5 %all-to-all-start.2 = ((bf16[32,8,2048]{2,0,1:T(8,128)(2,1)}), bf16[32,8,2048]{2,0,1:T(8,128)(2,1)S(1)}, u32[]{:S(2)}, u32[]{:S(2)}) async-start(bf16[32,8,2048]{2,0,1:T(8,128)(2,1)} %copy.46), calls=%async_computation.3 | async-start | bytes 2097152 | tf_op jit(solution)/shard_map/all_to_all | solution.py:166
  287.2 0.1 copy.40
  287.3 3.0 multiply_reduce_fusion.1
  290.3 1.0 multiply_convert_fusion.1
  291.3 21.4 %all-to-all-done.2 = bf16[32,8,2048]{2,0,1:T(8,128)(2,1)S(1)} async-done(((bf16[32,8,2048]{2,0,1:T(8,128)(2,1)}), bf16[32,8,2048]{2,0,1:T(8,128)(2,1)S(1)}, u32[]{:S(2)}, u32[]{:S(2)}) %all-to-all-start.2) | async-done | bytes 1048608 | tf_op jit(solution)/shard_map/all_to_all | solution.py:166
  312.7 0.6 copy.53
  313.3 0.9 gather_fusion.1
  314.2 0.7 reshape.287
  314.9 1.5 multiply_reduce_fusion
  316.4 0.1 multiply_reduce_fusion.2
  316.6 0.8 multiply_convert_fusion.2
  (67 shorter events, 0.6 us)
Async XLA Ops:
  7.2 192.5 %copy-start = (bf16[2048,256]{1,0:T(8,128)(2,1)S(1)}, bf16[2048,256]{1,0:T(8,128)(2,1)}, u32[]{:S(2)}) copy-start(bf16[2048,256]{1,0:T(8,128)(2,1)} %param.23) | copy-start | bytes 3145732
  7.2 31.8 %copy-start.2 = (bf16[256,2048]{1,0:T(8,128)(2,1)S(1)}, bf16[256,2048]{1,0:T(8,128)(2,1)}, u32[]{:S(2)}) copy-start(bf16[256,2048]{1,0:T(8,128)(2,1)} %param.28) | copy-start | bytes 3145732
  7.2 32.1 %copy-start.5 = (f32[2048]{0:T(1024)S(1)}, f32[2048]{0:T(1024)}, u32[]{:S(2)}) copy-start(f32[2048]{0:T(1024)} %param.31) | copy-start | bytes 24580
  7.2 102.5 %all-gather.5.cloned.1.call-start = ((), (), s32[]{:S(2)}) async-start(), calls=%async_computation.5 | async-start | bytes 5242880 | tf_op jit(solution)/shard_map/all_gather | solution.py:145
  76.1 147.6 %reduce-scatter.2.cloned.1.call-start = ((), (), s32[]{:S(2)}) async-start(), calls=%async_computation.4 | async-start | bytes 5242880 | tf_op jit(solution)/shard_map/reduce_scatter | solution.py:157
  109.7 7.5 %copy-start.10 = (bf16[128,8,2048]{2,1,0:T(8,128)(2,1)S(1)}, bf16[128,8,2048]{2,1,0:T(8,128)(2,1)}, u32[]{:S(2)}) copy-start(bf16[128,8,2048]{2,1,0:T(8,128)(2,1)} %all-gather.5.cloned.1.call-done) | copy-start | bytes 12582916
  109.7 7.5 %copy-start.11 = (bf16[1,2048,896]{2,1,0:T(8,128)(2,1)S(1)}, bf16[1,2048,896]{2,1,0:T(8,128)(2,1)}, u32[]{:S(2)}) copy-start(bf16[1,2048,896]{2,1,0:T(8,128)(2,1)} %param.32) | copy-start | bytes 11010052
  117.2 4.8 %copy-start.12 = (bf16[1,896,2048]{2,1,0:T(8,128)(2,1)S(1)}, bf16[1,896,2048]{2,1,0:T(8,128)(2,1)}, u32[]{:S(2)}) copy-start(bf16[1,896,2048]{2,1,0:T(8,128)(2,1)} %param.34) | copy-start | bytes 11010052
  128.0 1.6 copy-start.1
  128.0 2.1 copy-start.6
  128.0 4.3 %copy-start.3 = (bf16[2048,64]{0,1:T(8,128)(2,1)S(1)}, bf16[2048,64]{0,1:T(8,128)(2,1)}, u32[]{:S(2)}) copy-start(bf16[2048,64]{0,1:T(8,128)(2,1)} %param.24) | copy-start | bytes 786436
  130.1 35.5 %copy-start.4 = (bf16[2048,64]{0,1:T(8,128)(2,1)S(1)}, bf16[2048,64]{0,1:T(8,128)(2,1)}, u32[]{:S(2)}) copy-start(bf16[2048,64]{0,1:T(8,128)(2,1)} %param.25) | copy-start | bytes 786436
  219.4 67.7 %copy-start.9 = (f32[256,2]{0,1:T(2,128)S(1)}, f32[256,2]{0,1:T(2,128)}, u32[]{:S(2)}) copy-start(f32[256,2]{0,1:T(2,128)} %param.30) | copy-start | bytes 6148
  220.2 9.4 %all-to-all-start = ((bf16[4,128,256]{1,2,0:T(8,128)(2,1)}), bf16[4,128,256]{1,2,0:T(8,128)(2,1)S(1)}, u32[]{:S(2)}, u32[]{:S(2)}) async-start(bf16[4,128,256]{1,2,0:T(8,128)(2,1)} %copy.39), calls=%async_computation | async-start | bytes 524288 | tf_op jit(solution)/shard_map/all_to_all | solution.py:108
  226.5 63.9 %copy-start.7 = (f32[2048]{0:T(1024)S(1)}, f32[2048]{0:T(1024)}, u32[]{:S(2)}) copy-start(f32[2048]{0:T(1024)} %param.27) | copy-start | bytes 24580
  229.6 83.1 %all-to-all-start.2 = ((bf16[32,8,2048]{2,0,1:T(8,128)(2,1)}), bf16[32,8,2048]{2,0,1:T(8,128)(2,1)S(1)}, u32[]{:S(2)}, u32[]{:S(2)}) async-start(bf16[32,8,2048]{2,0,1:T(8,128)(2,1)} %copy.46), calls=%async_computation.3 | async-start | bytes 2097152 | tf_op jit(solution)/shard_map/all_to_all | solution.py:166
  313.3 3.3 %copy-start.8 = (f32[2048]{0:T(1024)S(1)}, f32[2048]{0:T(1024)}, u32[]{:S(2)}) copy-start(f32[2048]{0:T(1024)} %param.35) | copy-start | bytes 24580
Sparse Core Ops, SparseCore 0:
  76.2 33.4 all-gather.4
  128.1 44.5 reduce-scatter.1
where the time goes:
time: 326 us; the launch traced here: 324 us
  blocking collectives  95.8 us (29%)
  starting transfers between devices  61.1 us (19%)
  waiting for transfers between devices  58 us (18%)
  local copies, waits for them, and re-layouts  51.1 us (16%)
  matrix products  29 us (9%)
  between operations  14.4 us (4%)
  other arithmetic  9.24 us (3%)
  loops' own time  5.57 us (2%)
    all_to_all x1, starting transfers between devices, expert_half(): lax.all_to_all(results, 'ep', split_axis=1, concat_axis=1, tiled=True)  57.5 us
    all_gather x1, waiting for transfers between devices, expert_half(): slot_rows = lax.all_gather(arrived[None], 'tp', axis=0, tiled=True)  33.4 us
    all_to_all x1, blocking collectives, expert_half(): lax.all_to_all(outgoing, 'ep', split_axis=1, concat_axis=1, tiled=True)  32.9 us
    all_gather x1, blocking collectives, mixer_half(): key_piece = lax.all_gather(key_rows, 'ep', axis=0, tiled=True)  31.5 us
    all_gather x1, blocking collectives, mixer_half(): value_piece = lax.all_gather(value_rows, 'ep', axis=0, tiled=True)  31.4 us
    scatter x1, local copies, waits for them, and re-layouts, expert_half(): slot_table = jnp.full((quarters, slot_count, experts), row_count, jnp.int...  29.5 us
    all_to_all x1, waiting for transfers between devices, expert_half(): lax.all_to_all(results, 'ep', split_axis=1, concat_axis=1, tiled=True)  21.4 us
    dot_general x1, matrix products, expert_half(): up_part = jnp.dot(flat_rows, up_local, preferred_element_type=jnp.float32)  7.49 us
  transfers between devices with their start and end apart: 4, of which 3 were waited for; matrix products, arithmetic and copies ran while one was open for 9% of the time, Pallas kernels for 0%

commit v1 on v0

--- a/solution.py
+++ b/solution.py
@@ -58,8 +58,11 @@
         jnp.zeros((kv_local, group_size, row_count, HD), jnp.float32),
     )
     running = start_state
-    key_piece = lax.all_gather(key_rows, "ep", axis=0, tiled=True)
-    value_piece = lax.all_gather(value_rows, "ep", axis=0, tiled=True)
+    key_piece, value_piece = jnp.split(
+        lax.all_gather(jnp.concatenate([key_rows, value_rows], axis=1), "ep", axis=0, tiled=True),
+        [key_rows.shape[1]],
+        axis=1,
+    )
     piece_rows = key_piece.shape[0]
     block_rows = math.gcd(piece_rows, 512)
     block_total = piece_rows // block_rows

time: 326 us -> 262 us (0.80)
  blocking collectives: 95.8 us -> 32.9 us
  waiting for transfers between devices: 58 us -> 98.5 us
  starting transfers between devices: 61.1 us -> 22.1 us
    all_gather x2 -> x0, blocking collectives: 62.9 us -> none  [the longest x1 31.5 us: mixer_half(): key_piece = lax.all_gather(key_rows, 'ep', axis=0, tiled=True)]
    all_to_all x1, starting transfers between devices: 57.5 us -> 18.2 us  [expert_half(): lax.all_to_all(results, 'ep', split_axis=1, concat_axis=1, tiled=True)]
    reduce_scatter x1, waiting for transfers between devices: 0.02 us -> 27 us  [expert_half(): lax.psum_scatter(product.reshape(lax.axis_size('tp') * 1, slot_count, exp...]
    all_gather x0 -> x1, waiting for transfers between devices: none -> 21.6 us  [mixer_half(): lax.all_gather(jnp.concatenate([key_rows, value_rows], axis=1), 'ep', axi...]
    all_gather x1, waiting for transfers between devices: 33.4 us -> 28.4 us  [expert_half(): slot_rows = lax.all_gather(arrived[None], 'tp', axis=0, tiled=True)]
    unnamed x31 -> x30, local copies, waits for them, and re-layouts: 4.81 us -> 1.12 us
  transfers between devices with their start and end apart: 4 -> 5, of which waited for: 3 -> 4; matrix products, arithmetic and copies ran while one was open for 9% -> 17% of each run, Pallas kernels for 0% -> 0%
where the time goes in v1:
time: 262 us; the launch traced here: 261 us
  waiting for transfers between devices  98.5 us (38%)
  local copies, waits for them, and re-layouts  50.5 us (19%)
  blocking collectives  32.9 us (13%)
  matrix products  27.2 us (10%)
  starting transfers between devices  22.1 us (8%)
  between operations  14.1 us (5%)
  other arithmetic  9.88 us (4%)
  loops' own time  5.7 us (2%)
    all_to_all x1, blocking collectives, expert_half(): lax.all_to_all(outgoing, 'ep', split_axis=1, concat_axis=1, tiled=True)  32.9 us
    scatter x1, local copies, waits for them, and re-layouts, expert_half(): slot_table = jnp.full((quarters, slot_count, experts), row_count, jnp.int...  29.5 us
    all_gather x1, waiting for transfers between devices, expert_half(): slot_rows = lax.all_gather(arrived[None], 'tp', axis=0, tiled=True)  28.4 us
    reduce_scatter x1, waiting for transfers between devices, expert_half(): lax.psum_scatter(product.reshape(lax.axis_size('tp') * 1, slot_count, exp...  27 us
    all_gather x1, waiting for transfers between devices, mixer_half(): lax.all_gather(jnp.concatenate([key_rows, value_rows], axis=1), 'ep', axi...  21.6 us
    all_to_all x1, waiting for transfers between devices, expert_half(): lax.all_to_all(results, 'ep', split_axis=1, concat_axis=1, tiled=True)  21.4 us
    all_to_all x1, starting transfers between devices, expert_half(): lax.all_to_all(results, 'ep', split_axis=1, concat_axis=1, tiled=True)  18.2 us
    dot_general x1, matrix products, expert_half(): up_part = jnp.dot(flat_rows, up_local, preferred_element_type=jnp.float32)  7.49 us
  transfers between devices with their start and end apart: 5, of which 4 were waited for; matrix products, arithmetic and copies ran while one was open for 17% of the time, Pallas kernels for 0%

profile of v1, /device:TPU:0, one launch (start us, length us, event | category | flops | bytes accessed | tf_op | source)
XLA Modules:
  0.0 260.8 jit_solution(5046767718479833160)
XLA Ops:
  7.2 0.9 copy.41
  8.2 0.1 eq.15
  8.3 0.1 reshape.284
  8.5 0.1 fusion.48
  8.7 0.3 reduce_window_sum.11
  8.9 0.2 select_reduce_fusion
  9.2 29.5 %scatter_fusion = s32[4,32,8]{1,2,0:T(8,128)S(1)} fusion(s32[4,32,8]{1,2,0:T(8,128)S(1)} %broadcast_in_dim.39, s32[512]{0:T(512)S(1)} %fusion.54, s32[512]{0:T(512)S(1)} %fusion.56), kind=kCustom, calls=%fused_computation.2 | custom fusion | bytes 12288 | tf_op jit(solution)/shard_map/scatter | solution.py:139
  38.8 0.1 copy.43
  38.8 0.1 reshape.290
  39.0 0.3 fusion.43
  39.3 0.3 fusion.45
  39.6 0.1 concatenate.10
  39.7 2.3 gather_fusion
  42.0 2.0 copy.44
  44.0 32.9 %all_to_all.26 = bf16[32,8,2048]{2,0,1:T(8,128)(2,1)S(1)} all-to-all(bf16[32,8,2048]{2,0,1:T(8,128)(2,1)S(1)} %copy.44), channel_id=1, replica_groups=mesh['ep'=8,'tp'=4] {'ep'}, dimensions={1} | all-to-all | bytes 2097152 | tf_op jit(solution)/shard_map/all_to_all | solution.py:147
  76.8 1.6 copy.45
  78.5 0.5 fusion.29
  79.0 2.1 fusion.31
  81.1 0.8 fusion.46
  81.9 0.8 fusion.47
  82.7 0.7 pad_maximum_fusion
  83.4 0.2 reduce-scatter.2.cloned.1.call-start
  83.6 28.4 %all-gather.6.cloned.1.call-done = bf16[128,8,2048]{2,1,0:T(8,128)(2,1)} async-done(((bf16[32,8,2048]{2,1,0:T(8,128)(2,1)}), bf16[128,8,2048]{2,1,0:T(8,128)(2,1)}) %all-gather.6.cloned.1.call-update) | async-done | bytes 4194320 | tf_op jit(solution)/shard_map/all_gather | solution.py:148
  112.0 7.5 %fusion.32 = f32[1024,896]{1,0:T(8,128)S(1)} fusion(bf16[128,8,2048]{2,1,0:T(8,128)(2,1)} %all-gather.6.cloned.1.call-done, bf16[1,2048,896]{2,1,0:T(8,128)(2,1)} %param.33), kind=kOutput, calls=%fused_computation.40 | convolution fusion | flops 3758096384 | bytes 11534336 | tf_op jit(solution)/shard_map/dot_general | solution.py:151
  119.6 4.8 %multiply_convert_fusion = bf16[1024,896]{1,0:T(8,128)(2,1)S(1)} fusion(f32[1024,896]{1,0:T(8,128)S(1)} %fusion.32, bf16[1,2048,896]{2,1,0:T(8,128)(2,1)S(1)} %copy-done.11, bf16[128,8,2048]{2,1,0:T(8,128)(2,1)S(1)} %copy-done.10), kind=kOutput, calls=%fused_computation.48 | convolution fusion | flops 3763601408 | bytes 13369344 | tf_op jit(solution)/shard_map/dot_general | solution.py:150
  124.3 6.0 %convolution_convert_fusion = bf16[4,32,8,2048]{3,2,1,0:T(8,128)(2,1)} fusion(bf16[4,32,8,896]{3,2,1,0:T(8,128)(2,1)S(1)} %bitcast.161, bf16[1,896,2048]{2,1,0:T(8,128)(2,1)S(1)} %copy-done.12), kind=kOutput, calls=%fused_computation.44 | convolution fusion | flops 3760193536 | bytes 9699328 | tf_op jit(solution)/shard_map/dot_general | solution.py:157
  130.4 0.7 dynamic-slice_bitcast_fusion.1
  131.1 1.5 convolution_convert_fusion.1
  132.5 21.6 %all-gather.4.cloned.1.call-done = bf16[4096,2,64]{0,2,1:T(8,128)(2,1)} async-done(((bf16[512,2,64]{0,2,1:T(8,128)(2,1)}), bf16[4096,2,64]{0,2,1:T(8,128)(2,1)}) %all-gather.4.cloned.1.call-update) | async-done | bytes 1048592 | tf_op jit(solution)/shard_map/all_gather | solution.py:62
  154.1 1.3 fusion.65
  155.4 0.1 copy_bitcast_fusion.1
  155.6 15.9 %while.15 = (s32[]{:T(128)}, f32[1,4,512]{2,1,0:T(4,128)S(1)}, f32[1,4,512]{2,1,0:T(4,128)S(1)}, f32[1,4,512,64]{2,3,1,0:T(8,128)S(1)}, s32[8]{0:T(128)S(1)}, /*...) while((s32[]{:T(128)}, f32[1,4,512]{2,1,0:T(4,128)S(1)}, ...), condition=%wide.region_6.7_spmd.clone, body=%wide.region_1.6_spmd.clone.sunk | while | flops 288889856 | bytes 15282553 | solution.py:102
  155.6 0.6 dynamic_slice.79
  156.9 5.6 %conditional.3 = ((f32[1,4,512]{2,1,0:T(4,128)S(1)}, f32[1,4,512]{2,1,0:T(4,128)S(1)}, f32[1,4,512,64]{2,3,1,0:T(8,128)S(1)})) conditional(s32[]{:T(128)} %convert_element_type.127, (f32[1,4,512]{2,1,0:T(4,128)S(1)}, f32[1,4,512]{2,1,0:T(4,128)S(1)}, f32[1,4,512,64]{2,3,1,0:T(8,128)S(1)}) %tuple.50, (s32[]{:T(128)}, s32[]{:T(128)}, ...), branch_computations={%region_2.2_spmd, %region_3.5_spmd} | conditional | flops 288889856 | bytes 15280214 | solution.py:100
  156.9 0.8 dynamic-slice_bitcast_fusion
  157.7 0.2 broadcast_compare_fusion
  157.9 1.2 fusion.6
  159.1 1.7 fusion.14
  160.9 1.5 fusion.5
  162.4 0.6 dynamic_slice.79
  163.7 0.6 dynamic_slice.79
  165.0 0.6 dynamic_slice.79
  166.3 0.6 dynamic_slice.79
  167.6 0.6 dynamic_slice.79
  168.9 0.6 dynamic_slice.79
  170.2 0.6 dynamic_slice.79
  171.5 0.1 fusion.49
  171.6 0.1 convert_element_type.72
  171.6 0.7 copy.39
  172.4 3.6 %all-to-all-start = ((bf16[4,128,256]{1,2,0:T(8,128)(2,1)}), bf16[4,128,256]{1,2,0:T(8,128)(2,1)S(1)}, u32[]{:S(2)}, u32[]{:S(2)}) async-start(bf16[4,128,256]{1,2,0:T(8,128)(2,1)} %copy.39), calls=%async_computation | async-start | bytes 524288 | tf_op jit(solution)/shard_map/all_to_all | solution.py:111
  176.0 27.0 %reduce-scatter.2.cloned.1.call-done = bf16[1,32,8,2048]{3,2,1,0:T(8,128)(2,1)} async-done(((bf16[4,32,8,2048]{3,2,1,0:T(8,128)(2,1)}), bf16[1,32,8,2048]{3,2,1,0:T(8,128)(2,1)}) %reduce-scatter.2.cloned.1.call-update) | async-done | bytes 1048592 | tf_op jit(solution)/shard_map/reduce_scatter | solution.py:160
  203.1 2.8 %copy.46 = bf16[32,8,2048]{2,0,1:T(8,128)(2,1)} copy(bf16[32,8,2048]{2,1,0:T(8,128)(2,1)} %bitcast.155) | data formatting | bytes 2097152 | tf_op jit(solution)/shard_map/convert_element_type | solution.py:168
  205.8 18.2 %all-to-all-start.2 = ((bf16[32,8,2048]{2,0,1:T(8,128)(2,1)}), bf16[32,8,2048]{2,0,1:T(8,128)(2,1)S(1)}, u32[]{:S(2)}, u32[]{:S(2)}) async-start(bf16[32,8,2048]{2,0,1:T(8,128)(2,1)} %copy.46), calls=%async_computation.3 | async-start | bytes 2097152 | tf_op jit(solution)/shard_map/all_to_all | solution.py:169
  224.0 0.1 constant_dynamic-slice_fusion.2
  224.1 0.1 copy.40
  224.2 3.0 %multiply_reduce_fusion.1 = (f32[128]{0:T(128)S(1)}, f32[128,2048]{1,0:T(8,128)S(1)}) fusion(bf16[128,1024]{0,1:T(8,128)(2,1)S(1)} %bitcast.154, bf16[1024,2048]{1,0:T(8,128)(2,1)} %param.26), kind=kOutput, calls=%fused_computation.62 | convolution fusion | flops 537395072 | bytes 5505536 | tf_op jit(solution)/shard_map/dot_general | solution.py:112
  227.2 1.0 multiply_convert_fusion.1
  228.2 21.4 %all-to-all-done.2 = bf16[32,8,2048]{2,0,1:T(8,128)(2,1)S(1)} async-done(((bf16[32,8,2048]{2,0,1:T(8,128)(2,1)}), bf16[32,8,2048]{2,0,1:T(8,128)(2,1)S(1)}, u32[]{:S(2)}, u32[]{:S(2)}) %all-to-all-start.2) | async-done | bytes 1048608 | tf_op jit(solution)/shard_map/all_to_all | solution.py:169
  249.6 0.6 copy.55
  250.2 0.9 gather_fusion.1
  251.1 0.7 reshape.287
  251.8 1.5 multiply_reduce_fusion
  253.3 0.1 multiply_reduce_fusion.2
  253.5 0.8 multiply_convert_fusion.2
  (69 shorter events, 0.5 us)
Async XLA Ops:
  7.2 123.9 %copy-start = (bf16[2048,256]{1,0:T(8,128)(2,1)S(1)}, bf16[2048,256]{1,0:T(8,128)(2,1)}, u32[]{:S(2)}) copy-start(bf16[2048,256]{1,0:T(8,128)(2,1)} %param.23) | copy-start | bytes 3145732
  7.2 31.8 %copy-start.2 = (bf16[256,2048]{1,0:T(8,128)(2,1)S(1)}, bf16[256,2048]{1,0:T(8,128)(2,1)}, u32[]{:S(2)}) copy-start(bf16[256,2048]{1,0:T(8,128)(2,1)} %param.28) | copy-start | bytes 3145732
  7.2 32.1 %copy-start.5 = (f32[2048]{0:T(1024)S(1)}, f32[2048]{0:T(1024)}, u32[]{:S(2)}) copy-start(f32[2048]{0:T(1024)} %param.31) | copy-start | bytes 24580
  7.2 104.8 %all-gather.6.cloned.1.call-start = ((), (), s32[]{:S(2)}) async-start(), calls=%async_computation.6 | async-start | bytes 5242880 | tf_op jit(solution)/shard_map/all_gather | solution.py:148
  42.0 36.5 %copy-start.1 = (bf16[512,2048]{1,0:T(8,128)(2,1)S(1)}, bf16[512,2048]{1,0:T(8,128)(2,1)}, u32[]{:S(2)}) copy-start(bf16[512,2048]{1,0:T(8,128)(2,1)} %param.20) | copy-start | bytes 6291460
  44.0 35.0 %copy-start.6 = (f32[2048]{0:T(1024)S(1)}, f32[2048]{0:T(1024)}, u32[]{:S(2)}) copy-start(f32[2048]{0:T(1024)} %param.22) | copy-start | bytes 24580
  78.4 2.7 %copy-start.3 = (bf16[2048,64]{0,1:T(8,128)(2,1)S(1)}, bf16[2048,64]{0,1:T(8,128)(2,1)}, u32[]{:S(2)}) copy-start(bf16[2048,64]{0,1:T(8,128)(2,1)} %param.24) | copy-start | bytes 786436
  78.4 75.7 %all-gather.4.cloned.1.call-start = ((), (), s32[]{:S(2)}) async-start(), calls=%async_computation.4 | async-start | bytes 1179648 | tf_op jit(solution)/shard_map/all_gather | solution.py:62
  78.5 3.4 %copy-start.4 = (bf16[2048,64]{0,1:T(8,128)(2,1)S(1)}, bf16[2048,64]{0,1:T(8,128)(2,1)}, u32[]{:S(2)}) copy-start(bf16[2048,64]{0,1:T(8,128)(2,1)} %param.25) | copy-start | bytes 786436
  83.4 119.7 %reduce-scatter.2.cloned.1.call-start = ((), (), s32[]{:S(2)}) async-start(), calls=%async_computation.5 | async-start | bytes 5242880 | tf_op jit(solution)/shard_map/reduce_scatter | solution.py:160
  112.0 7.5 %copy-start.10 = (bf16[128,8,2048]{2,1,0:T(8,128)(2,1)S(1)}, bf16[128,8,2048]{2,1,0:T(8,128)(2,1)}, u32[]{:S(2)}) copy-start(bf16[128,8,2048]{2,1,0:T(8,128)(2,1)} %all-gather.6.cloned.1.call-done) | copy-start | bytes 12582916
  112.0 7.5 %copy-start.11 = (bf16[1,2048,896]{2,1,0:T(8,128)(2,1)S(1)}, bf16[1,2048,896]{2,1,0:T(8,128)(2,1)}, u32[]{:S(2)}) copy-start(bf16[1,2048,896]{2,1,0:T(8,128)(2,1)} %param.32) | copy-start | bytes 11010052
  119.6 4.8 %copy-start.12 = (bf16[1,896,2048]{2,1,0:T(8,128)(2,1)S(1)}, bf16[1,896,2048]{2,1,0:T(8,128)(2,1)}, u32[]{:S(2)}) copy-start(bf16[1,896,2048]{2,1,0:T(8,128)(2,1)} %param.34) | copy-start | bytes 11010052
  132.5 23.0 %copy-start.13 = (bf16[512,256]{0,1:T(8,128)(2,1)S(1)}, bf16[512,256]{0,1:T(8,128)(2,1)}, u32[]{:S(2)}) copy-start(bf16[512,256]{0,1:T(8,128)(2,1)} %convolution_convert_fusion.1) | copy-start | bytes 786436
  171.5 52.5 %copy-start.9 = (f32[256,2]{0,1:T(2,128)S(1)}, f32[256,2]{0,1:T(2,128)}, u32[]{:S(2)}) copy-start(f32[256,2]{0,1:T(2,128)} %param.30) | copy-start | bytes 6148
  172.4 33.5 %all-to-all-start = ((bf16[4,128,256]{1,2,0:T(8,128)(2,1)}), bf16[4,128,256]{1,2,0:T(8,128)(2,1)S(1)}, u32[]{:S(2)}, u32[]{:S(2)}) async-start(bf16[4,128,256]{1,2,0:T(8,128)(2,1)} %copy.39), calls=%async_computation | async-start | bytes 524288 | tf_op jit(solution)/shard_map/all_to_all | solution.py:111
  205.8 21.4 %copy-start.7 = (f32[2048]{0:T(1024)S(1)}, f32[2048]{0:T(1024)}, u32[]{:S(2)}) copy-start(f32[2048]{0:T(1024)} %param.27) | copy-start | bytes 24580
  205.8 43.8 %all-to-all-start.2 = ((bf16[32,8,2048]{2,0,1:T(8,128)(2,1)}), bf16[32,8,2048]{2,0,1:T(8,128)(2,1)S(1)}, u32[]{:S(2)}, u32[]{:S(2)}) async-start(bf16[32,8,2048]{2,0,1:T(8,128)(2,1)} %copy.46), calls=%async_computation.3 | async-start | bytes 2097152 | tf_op jit(solution)/shard_map/all_to_all | solution.py:169
  250.2 3.3 %copy-start.8 = (f32[2048]{0:T(1024)S(1)}, f32[2048]{0:T(1024)}, u32[]{:S(2)}) copy-start(f32[2048]{0:T(1024)} %param.35) | copy-start | bytes 24580
Sparse Core Ops, SparseCore 0:
  78.5 33.4 all-gather.5
  114.6 39.4 all-gather.3
  156.6 46.3 reduce-scatter.1
